TPU v7x, 32 devices: a whole 2x2x4 slice. The times are simulated.
32 devices in a mesh: gr: 2 (over core), sp: 8 (over z, y), tp: 2 (over x).
Axes of the slice: x: 2, y: 2, z: 4, core: 2. Of those that a mesh axis runs over, the one named last changes fastest.
Arguments:
- mixer_input: bfloat16 [16, 1536, 2048], P(('gr', 'tp'), 'sp'), may hold values from -16.8 to 16.8
- key_weight: bfloat16 [2048, 256], P('tp'), may hold values from -0.125 to 0.125
- content_projection_matrix: bfloat16 [2048, 256], P('tp'), may hold values from -0.125 to 0.125
- new_queries: bfloat16 [16, 32, 64], P(('gr', 'sp'), 'tp'), may hold values from -6 to 6
- head_stick_offset: float32 [32], replicated, may hold values from -11 to -4
Outputs:
- kv_cache: bfloat16 [16, 4, 1536, 128], P(('gr', 'sp'), 'tp')
- initial_attended_output: bfloat16 [16, 32, 64], P(('gr', 'sp'), 'tp')
All inputs are finite; a program needn't handle non-finite values.
Results may differ from a plain program's by a relative error of at most 0.0081.
Values may be sent and summed in bfloat16 or wider, within the bound.
A program may use at most 64 MiB of HBM per device.

v0:
```python
import jax
import jax.numpy as jnp
from jax import lax
from jax.sharding import PartitionSpec as P

HEAD_DIM = 64


def local(mixer_input, key_weight, content_projection_matrix, new_queries, head_stick_offset):
    group_seqs, block_rows, model_width = mixer_input.shape
    key_heads = key_weight.shape[1] // HEAD_DIM
    head_devices = lax.axis_size("tp")
    copies = max(1, head_devices // key_heads)
    input_rows = mixer_input.reshape(group_seqs * block_rows, model_width)
    key_sum = jnp.dot(
        input_rows,
        lax.all_gather(key_weight, "tp", axis=0, tiled=True),
        preferred_element_type=jnp.float32,
    )
    value_sum = jnp.dot(
        input_rows,
        lax.all_gather(content_projection_matrix, "tp", axis=0, tiled=True),
        preferred_element_type=jnp.float32,
    )
    key_rows = key_sum.astype(jnp.bfloat16).reshape(group_seqs, block_rows, key_heads, HEAD_DIM)
    value_rows = value_sum.astype(jnp.bfloat16).reshape(group_seqs, block_rows, key_heads, HEAD_DIM)
    stacked = jnp.concatenate([key_rows, value_rows], axis=3).transpose(0, 2, 1, 3)
    spread = jnp.repeat(stacked, copies, axis=1)
    spread = lax.all_to_all(spread, "tp", split_axis=1, concat_axis=0, tiled=True)
    kv_cache = lax.all_to_all(spread, "sp", split_axis=0, concat_axis=2, tiled=True)
    seq_local = kv_cache.shape[0]
    slot_local = kv_cache.shape[1]
    head_local = new_queries.shape[1]
    inverse_root = HEAD_DIM ** (-0.5)
    offset_values = lax.dynamic_slice_in_dim(
        head_stick_offset, lax.axis_index("tp") * head_local, head_local
    )
    grouped = new_queries.reshape(seq_local, slot_local, head_local // slot_local, HEAD_DIM)
    cache_keys = kv_cache[:, :, :, :HEAD_DIM]
    cache_values = kv_cache[:, :, :, HEAD_DIM:]
    logit_scores = (
        jnp.einsum("bhgd,bhsd->bhgs", grouped, cache_keys, preferred_element_type=jnp.float32)
        * inverse_root
    )
    logit_scores = logit_scores + offset_values.reshape(1, slot_local, -1, 1)
    stay_terms = jax.nn.log_sigmoid(-logit_scores)
    later_terms = lax.cumsum(stay_terms, axis=3, reverse=True) - stay_terms
    weights = jnp.exp(jax.nn.log_sigmoid(logit_scores) + later_terms).astype(jnp.bfloat16)
    result = jnp.einsum(
        "bhgs,bhsd->bhgd", weights, cache_values, preferred_element_type=jnp.float32
    )
    initial_attended_output = result.reshape(seq_local, head_local, HEAD_DIM).astype(jnp.bfloat16)
    return (kv_cache, initial_attended_output)


def solution(mesh):
    return jax.shard_map(
        local,
        mesh=mesh,
        in_specs=(
            P(("gr", "tp"), "sp", None),
            P("tp", None),
            P("tp", None),
            P(("gr", "sp"), "tp", None),
            P(),
        ),
        out_specs=(P(("gr", "sp"), "tp", None, None), P(("gr", "sp"), "tp", None)),
        check_vma=False,
    )
```

profile of v0, /device:TPU:0, one launch (start us, length us, event | category | flops | bytes accessed | tf_op | source)
XLA Modules:
  0.0 139.1 jit_solution(8693301563375391553)
XLA Ops:
  7.2 0.0 copy-start
  7.2 0.0 all-gather.5.cloned.1.call-start
  7.2 0.7 all-gather.5.cloned.1.call-update
  7.9 0.0 all-gather.3.cloned.1.call-start
  8.0 0.7 all-gather.3.cloned.1.call-update
  8.7 24.9 %all-gather.5.cloned.1.call-done = bf16[2048,256]{1,0:T(8,128)(2,1)} async-done(((bf16[1024,256]{1,0:T(8,128)(2,1)}), bf16[2048,256]{1,0:T(8,128)(2,1)}) %all-gather.5.cloned.1.call-update) | async-done | bytes 1048592 | tf_op jit(solution)/shard_map/all_gather | solution.py:22
  33.6 0.0 copy-done
  33.6 3.0 %convolution_convert_fusion = bf16[768,256]{1,0:T(8,128)(2,1)} fusion(bf16[768,2048]{1,0:T(8,128)(2,1)S(1)} %bitcast.47, bf16[2048,256]{1,0:T(8,128)(2,1)} %all-gather.5.cloned.1.call-done), kind=kOutput, calls=%fused_computation.3 | convolution fusion | flops 805502976 | bytes 4587520 | tf_op jit(solution)/shard_map/dot_general | solution.py:20
  36.5 1.2 copy.28
  37.7 1.3 reshape.94
  39.0 17.5 %all-gather.3.cloned.1.call-done = bf16[2048,256]{1,0:T(8,128)(2,1)} async-done(((bf16[1024,256]{1,0:T(8,128)(2,1)}), bf16[2048,256]{1,0:T(8,128)(2,1)}) %all-gather.3.cloned.1.call-update) | async-done | bytes 1048592 | tf_op jit(solution)/shard_map/all_gather | solution.py:17
  56.4 3.0 %convolution_convert_fusion.1 = bf16[768,256]{1,0:T(8,128)(2,1)} fusion(bf16[768,2048]{1,0:T(8,128)(2,1)S(1)} %bitcast.46, bf16[2048,256]{1,0:T(8,128)(2,1)} %all-gather.3.cloned.1.call-done), kind=kOutput, calls=%fused_computation.4 | convolution fusion | flops 805502976 | bytes 4587520 | tf_op jit(solution)/shard_map/dot_general | solution.py:15
  59.4 1.2 copy.27
  60.6 1.3 reshape.93
  61.8 2.9 %maximum_bitcast_fusion = bf16[4,4,192,128]{2,0,3,1:T(4,128)(2,1)} fusion(bf16[4,192,4,64]{1,0,3,2:T(4,128)(2,1)} %reshape.94, bf16[4,192,4,64]{1,0,3,2:T(4,128)(2,1)} %reshape.93), kind=kLoop, calls=%fused_computation.7 | loop fusion | flops 393216 | bytes 1572864 | tf_op jit(solution)/shard_map/transpose | solution.py:27
  64.8 0.0 copy-start.3
  64.8 2.3 %copy.29 = bf16[4,4,192,128]{3,2,0,1:T(8,128)(2,1)} copy(bf16[4,4,192,128]{2,0,3,1:T(4,128)(2,1)} %maximum_bitcast_fusion) | data formatting | bytes 1572864 | tf_op jit(solution)/shard_map/transpose | solution.py:27
  67.1 0.0 copy-start.2
  67.1 14.5 %all_to_all.36 = bf16[4,4,192,128]{3,2,0,1:T(8,128)(2,1)S(1)} all-to-all(bf16[4,4,192,128]{3,2,0,1:T(8,128)(2,1)} %copy.29), channel_id=1, replica_groups=mesh['gr'=2,'sp'=8,'tp'=2] {'tp'}, dimensions={1} | all-to-all | bytes 1572864 | tf_op jit(solution)/shard_map/all_to_all | solution.py:29
  81.6 0.9 copy.31
  82.6 5.5 %all-to-all-start.1 = ((bf16[8,2,192,128]{3,2,1,0:T(8,128)(2,1)}), bf16[8,2,192,128]{3,2,1,0:T(8,128)(2,1)}, u32[]{:S(2)}, u32[]{:S(2)}) async-start(bf16[8,2,192,128]{3,2,1,0:T(8,128)(2,1)} %bitcast.48), calls=%async_computation.1 | async-start | bytes 1572864 | tf_op jit(solution)/shard_map/all_to_all | solution.py:30
  88.1 0.0 copy-done.3
  88.1 0.1 dynamic_slice.3
  88.2 0.1 add.32
  88.3 19.2 %all-to-all-done.1 = bf16[8,2,192,128]{3,2,1,0:T(8,128)(2,1)} async-done(((bf16[8,2,192,128]{3,2,1,0:T(8,128)(2,1)}), bf16[8,2,192,128]{3,2,1,0:T(8,128)(2,1)}, u32[]{:S(2)}, u32[]{:S(2)}) %all-to-all-start.1) | async-done | bytes 786464 | tf_op jit(solution)/shard_map/all_to_all | solution.py:30
  107.4 1.2 copy.32
  108.6 0.0 copy-start.1
  108.6 0.0 copy-done.2
  108.6 0.3 fusion.1
  108.9 0.1 fusion.13
  109.0 0.5 copy-done.1
  109.5 19.9 %reduce-window.6 = f32[1,2,8,12,128]{4,3,2,1,0:T(8,128)S(1)} reduce-window(f32[1,2,8,12,128]{4,3,2,1,0:T(8,128)S(1)} %copy.34, f32[]{:T(128)} %constant.18.clone.1), window={size=1x1x1x1x128 pad=0_0x0_0x0_0x0_0x0_127}, to_apply=%region_0.1 | reduce-window | flops 3121152 | bytes 196612 | tf_op jit(solution)/shard_map/reduce-window
  129.4 0.1 slice_reduce_fusion
  129.5 0.3 reduce-window.9
  129.9 0.1 slice_bitcast_fusion.4
  129.9 0.1 copy.35
  130.0 2.2 %fusion.2 = bf16[1,16,64]{2,1,0:T(8,128)(2,1)} fusion(bf16[1,2,1536,128]{3,2,1,0:T(8,128)(2,1)} %bitcast.51, f32[2,8,1536]{2,1,0:T(8,128)S(1)} %reshape.98, f32[2,8,1536]{2,1,0:T(8,128)S(1)} %fusion.1, f32[2,8,12]{1,2,0:T(8,128)S(1)} %copy.35), kind=kOutput, calls=%fused_computation.6 | convolution fusion | flops 3613696 | bytes 985856 | tf_op jit(solution)/shard_map/bhgs,bhsd->bhgd/dot_general | solution.py:49
  (2 shorter events, 0.0 us)
Async XLA Ops:
  7.2 26.4 %copy-start = (bf16[4,192,2048]{2,1,0:T(8,128)(2,1)S(1)}, bf16[4,192,2048]{2,1,0:T(8,128)(2,1)}, u32[]{:S(2)}) copy-start(bf16[4,192,2048]{2,1,0:T(8,128)(2,1)} %param.5) | copy-start | bytes 9437188
  7.2 26.4 %all-gather.5.cloned.1.call-start = ((), (), s32[]{:S(2)}) async-start(), calls=%async_computation.3 | async-start | bytes 1572864 | tf_op jit(solution)/shard_map/all_gather | solution.py:22
  7.9 48.5 %all-gather.3.cloned.1.call-start = ((), (), s32[]{:S(2)}) async-start(), calls=%async_computation.2 | async-start | bytes 1572864 | tf_op jit(solution)/shard_map/all_gather | solution.py:17
  64.8 23.3 %copy-start.3 = (f32[32]{0:T(128)S(1)}, f32[32]{0:T(128)}, u32[]{:S(2)}) copy-start(f32[32]{0:T(128)} %param.9) | copy-start | bytes 388
  67.1 41.5 %copy-start.2 = (bf16[1,16,64]{2,1,0:T(8,128)(2,1)S(1)}, bf16[1,16,64]{2,1,0:T(8,128)(2,1)}, u32[]{:S(2)}) copy-start(bf16[1,16,64]{2,1,0:T(8,128)(2,1)} %param.8) | copy-start | bytes 6148
  82.6 24.8 %all-to-all-start.1 = ((bf16[8,2,192,128]{3,2,1,0:T(8,128)(2,1)}), bf16[8,2,192,128]{3,2,1,0:T(8,128)(2,1)}, u32[]{:S(2)}, u32[]{:S(2)}) async-start(bf16[8,2,192,128]{3,2,1,0:T(8,128)(2,1)} %bitcast.48), calls=%async_computation.1 | async-start | bytes 1572864 | tf_op jit(solution)/shard_map/all_to_all | solution.py:30
  108.6 0.9 copy-start.1
Sparse Core Ops, SparseCore 0:
  9.5 23.9 all-gather.4
  35.1 21.2 all-gather.2
where the time goes:
time: 140 us; the launch traced here: 139 us
  waiting for transfers between devices  62.9 us (45%)
  other arithmetic  23.2 us (17%)
  blocking collectives  14.5 us (10%)
  between operations  14.1 us (10%)
  local copies, waits for them, and re-layouts  10.3 us (7%)
  matrix products  8.45 us (6%)
  starting transfers between devices  5.59 us (4%)
    all_gather x1, waiting for transfers between devices, local(): lax.all_gather(content_projection_matrix, 'tp', axis=0, tiled=True)  24.9 us
    another operation x2, other arithmetic  20.2 us
    all_to_all x1, waiting for transfers between devices, local(): lax.all_to_all(spread, 'sp', split_axis=0, concat_axis=2, tiled=True)  19.2 us
    all_gather x1, waiting for transfers between devices, local(): lax.all_gather(key_weight, 'tp', axis=0, tiled=True)  17.5 us
    all_to_all x1, blocking collectives, local(): lax.all_to_all(spread, 'tp', split_axis=1, concat_axis=0, tiled=True)  14.5 us
    all_to_all x1, starting transfers between devices, local(): lax.all_to_all(spread, 'sp', split_axis=0, concat_axis=2, tiled=True)  5.52 us
    dot_general x1, matrix products, local(): jnp.dot(input_rows, lax.all_gather(key_weight, 'tp', axis=0, tiled=True),...  2.96 us
    dot_general x1, matrix products, local(): jnp.dot(input_rows, lax.all_gather(content_projection_matrix, 'tp', axis=...  2.95 us
  transfers between devices with their start and end apart: 3, of which 3 were waited for; matrix products, arithmetic and copies ran while one was open for 4% of the time, Pallas kernels for 0%

commit v1 on v0

--- a/solution.py
+++ b/solution.py
@@ -1,9 +1,20 @@
+import functools
 import jax
 import jax.numpy as jnp
 from jax import lax
 from jax.sharding import PartitionSpec as P
 
 HEAD_DIM = 64
+
+
+def windows_end(payload, in_dim):
+    t1 = jnp.stack([payload for _ in range(lax.axis_size("tp"))], axis=0)
+    high = lax.all_to_all(t1, "tp", split_axis=0, concat_axis=0)
+    s_next = jnp.concatenate(high, axis=in_dim)
+    return s_next
+
+
+name_target = functools.partial(windows_end, in_dim=0)
 
 
 def local(mixer_input, key_weight, content_projection_matrix, new_queries, head_stick_offset):
@@ -18,9 +29,7 @@
         preferred_element_type=jnp.float32,
     )
     value_sum = jnp.dot(
-        input_rows,
-        lax.all_gather(content_projection_matrix, "tp", axis=0, tiled=True),
-        preferred_element_type=jnp.float32,
+        input_rows, name_target(content_projection_matrix), preferred_element_type=jnp.float32
     )
     key_rows = key_sum.astype(jnp.bfloat16).reshape(group_seqs, block_rows, key_heads, HEAD_DIM)
     value_rows = value_sum.astype(jnp.bfloat16).reshape(group_seqs, block_rows, key_heads, HEAD_DIM)

time: 140 us -> 123 us (0.88)
  waiting for transfers between devices: 62.9 us -> 22.9 us
  blocking collectives: 14.5 us -> 38.8 us
  matrix products: 8.45 us -> 6.58 us
  other arithmetic: 23.2 us -> 24.7 us
    all_gather x1 -> x0, waiting for transfers between devices: 24.9 us -> none  [local(): lax.all_gather(content_projection_matrix, 'tp', axis=0, tiled=True)]
    all_to_all x0 -> x1, blocking collectives: none -> 23.9 us  [windows_end(): high = lax.all_to_all(t1, 'tp', split_axis=0, concat_axis=0)]
    all_gather x1, waiting for transfers between devices: 17.5 us -> 2.81 us  [local(): lax.all_gather(key_weight, 'tp', axis=0, tiled=True)]
    dot_general x1, matrix products: 2.95 us -> 1.08 us  [local(): jnp.dot(input_rows, name_target(content_projection_matrix), preferred_ele...]
    another operation x2 -> x3, other arithmetic: 20.2 us -> 21.7 us
  transfers between devices with their start and end apart: 3 -> 2, of which waited for: 3 -> 2; matrix products, arithmetic and copies ran while one was open for 4% -> 3% of each run, Pallas kernels for 0% -> 0%
where the time goes in v1:
time: 123 us; the launch traced here: 122 us
  blocking collectives  38.8 us (32%)
  other arithmetic  24.7 us (20%)
  waiting for transfers between devices  22.9 us (19%)
  between operations  14.1 us (11%)
  local copies, waits for them, and re-layouts  9.13 us (7%)
  matrix products  6.58 us (5%)
  starting transfers between devices  6.05 us (5%)
    all_to_all x1, blocking collectives, windows_end(): high = lax.all_to_all(t1, 'tp', split_axis=0, concat_axis=0)  23.9 us
    another operation x2, other arithmetic  20.2 us
    all_to_all x1, waiting for transfers between devices, local(): lax.all_to_all(spread, 'sp', split_axis=0, concat_axis=2, tiled=True)  19.4 us
    all_to_all x1, blocking collectives, local(): lax.all_to_all(spread, 'tp', split_axis=1, concat_axis=0, tiled=True)  14.8 us
    all_to_all x1, starting transfers between devices, local(): lax.all_to_all(spread, 'sp', split_axis=0, concat_axis=2, tiled=True)  6.02 us
    dot_general x1, matrix products, local(): jnp.dot(input_rows, lax.all_gather(key_weight, 'tp', axis=0, tiled=True),...  2.97 us
    transpose x1, other arithmetic, local(): jnp.concatenate([key_rows, value_rows], axis=3).transpose(0, 2, 1, 3)  2.93 us
    all_gather x1, waiting for transfers between devices, local(): lax.all_gather(key_weight, 'tp', axis=0, tiled=True)  2.81 us
  transfers between devices with their start and end apart: 2, of which 2 were waited for; matrix products, arithmetic and copies ran while one was open for 3% of the time, Pallas kernels for 0%

profile of v1, /device:TPU:0, one launch (start us, length us, event | category | flops | bytes accessed | tf_op | source)
XLA Modules:
  0.0 122.3 jit_solution(17469100163868614885)
XLA Ops:
  7.2 0.0 copy-start
  7.2 0.0 all-gather.2.cloned.1.call-start
  7.2 0.7 all-gather.2.cloned.1.call-update
  7.9 1.5 %pad_maximum_fusion = bf16[2,1024,256]{2,1,0:T(8,128)(2,1)S(1)} fusion(bf16[1,1024,256]{2,1,0:T(8,128)(2,1)} %bitcast.58), kind=kLoop, calls=%fused_computation.8 | loop fusion | flops 524288 | bytes 1572864 | tf_op jit(solution)/shard_map/stack | solution.py:11
  9.4 23.9 %all_to_all.41 = bf16[2,1024,256]{2,1,0:T(8,128)(2,1)S(1)} all-to-all(bf16[2,1024,256]{2,1,0:T(8,128)(2,1)S(1)} %pad_maximum_fusion), channel_id=1, replica_groups=mesh['gr'=2,'sp'=8,'tp'=2] {'tp'}, dimensions={0} | all-to-all | bytes 2097152 | tf_op jit(solution)/shard_map/all_to_all | solution.py:12
  33.4 0.0 copy-done
  33.4 1.1 fusion.2
  34.5 1.3 %reshape.98 = bf16[4,192,4,64]{1,0,3,2:T(4,128)(2,1)} reshape(bf16[768,256]{0,1:T(8,128)(2,1)S(1)} %fusion.2) | data formatting | bytes 786432 | tf_op jit(solution)/shard_map/reshape | solution.py:35
  35.7 2.8 %all-gather.2.cloned.1.call-done = bf16[2048,256]{1,0:T(8,128)(2,1)} async-done(((bf16[1024,256]{1,0:T(8,128)(2,1)}), bf16[2048,256]{1,0:T(8,128)(2,1)}) %all-gather.2.cloned.1.call-update) | async-done | bytes 1048592 | tf_op jit(solution)/shard_map/all_gather | solution.py:28
  38.5 3.0 %convolution_convert_fusion.1 = bf16[768,256]{1,0:T(8,128)(2,1)} fusion(bf16[768,2048]{1,0:T(8,128)(2,1)S(1)} %bitcast.50, bf16[2048,256]{1,0:T(8,128)(2,1)} %all-gather.2.cloned.1.call-done), kind=kOutput, calls=%fused_computation.4 | convolution fusion | flops 805502976 | bytes 4587520 | tf_op jit(solution)/shard_map/dot_general | solution.py:26
  41.5 1.2 copy.26
  42.7 1.3 %reshape.96 = bf16[4,192,4,64]{1,0,3,2:T(4,128)(2,1)} reshape(bf16[768,256]{0,1:T(8,128)(2,1)S(1)} %copy.26) | data formatting | bytes 786432 | tf_op jit(solution)/shard_map/reshape | solution.py:34
  44.0 2.9 %maximum_bitcast_fusion = bf16[4,4,192,128]{2,0,3,1:T(4,128)(2,1)} fusion(bf16[4,192,4,64]{1,0,3,2:T(4,128)(2,1)} %reshape.98, bf16[4,192,4,64]{1,0,3,2:T(4,128)(2,1)} %reshape.96), kind=kLoop, calls=%fused_computation.9 | loop fusion | flops 393216 | bytes 1572864 | tf_op jit(solution)/shard_map/transpose | solution.py:36
  46.9 0.0 copy-start.3
  46.9 2.3 %copy.27 = bf16[4,4,192,128]{3,2,0,1:T(8,128)(2,1)} copy(bf16[4,4,192,128]{2,0,3,1:T(4,128)(2,1)} %maximum_bitcast_fusion) | data formatting | bytes 1572864 | tf_op jit(solution)/shard_map/transpose | solution.py:36
  49.2 0.0 copy-start.2
  49.2 14.8 %all_to_all.42 = bf16[4,4,192,128]{3,2,0,1:T(8,128)(2,1)S(1)} all-to-all(bf16[4,4,192,128]{3,2,0,1:T(8,128)(2,1)} %copy.27), channel_id=1, replica_groups=mesh['gr'=2,'sp'=8,'tp'=2] {'tp'}, dimensions={1} | all-to-all | bytes 1572864 | tf_op jit(solution)/shard_map/all_to_all | solution.py:38
  64.1 0.9 copy.29
  65.0 6.0 %all-to-all-start.2 = ((bf16[8,2,192,128]{3,2,1,0:T(8,128)(2,1)}), bf16[8,2,192,128]{3,2,1,0:T(8,128)(2,1)}, u32[]{:S(2)}, u32[]{:S(2)}) async-start(bf16[8,2,192,128]{3,2,1,0:T(8,128)(2,1)} %bitcast.52), calls=%async_computation.2 | async-start | bytes 1572864 | tf_op jit(solution)/shard_map/all_to_all | solution.py:39
  71.0 0.0 copy-done.3
  71.0 0.1 dynamic_slice.3
  71.1 0.1 add.32
  71.2 19.4 %all-to-all-done.2 = bf16[8,2,192,128]{3,2,1,0:T(8,128)(2,1)} async-done(((bf16[8,2,192,128]{3,2,1,0:T(8,128)(2,1)}), bf16[8,2,192,128]{3,2,1,0:T(8,128)(2,1)}, u32[]{:S(2)}, u32[]{:S(2)}) %all-to-all-start.2) | async-done | bytes 786464 | tf_op jit(solution)/shard_map/all_to_all | solution.py:39
  90.6 1.2 copy.30
  91.8 0.0 copy-start.1
  91.8 0.0 copy-done.2
  91.8 0.3 fusion.1
  92.1 0.1 fusion.14
  92.2 0.5 copy-done.1
  92.7 19.9 %reduce-window.6 = f32[1,2,8,12,128]{4,3,2,1,0:T(8,128)S(1)} reduce-window(f32[1,2,8,12,128]{4,3,2,1,0:T(8,128)S(1)} %copy.32, f32[]{:T(128)} %constant.18.clone.1), window={size=1x1x1x1x128 pad=0_0x0_0x0_0x0_0x0_127}, to_apply=%region_0.1 | reduce-window | flops 3121152 | bytes 196612 | tf_op jit(solution)/shard_map/reduce-window
  112.6 0.1 slice_reduce_fusion
  112.7 0.3 reduce-window.9
  113.1 0.1 slice_bitcast_fusion.4
  113.1 0.1 copy.33
  113.2 2.2 %fusion.3 = bf16[1,16,64]{2,1,0:T(8,128)(2,1)} fusion(bf16[1,2,1536,128]{3,2,1,0:T(8,128)(2,1)} %bitcast.56, f32[2,8,1536]{2,1,0:T(8,128)S(1)} %reshape.102, f32[2,8,1536]{2,1,0:T(8,128)S(1)} %fusion.1, f32[2,8,12]{1,2,0:T(8,128)S(1)} %copy.33), kind=kOutput, calls=%fused_computation.7 | convolution fusion | flops 3613696 | bytes 985856 | tf_op jit(solution)/shard_map/bhgs,bhsd->bhgd/dot_general | solution.py:58
  (2 shorter events, 0.0 us)
Async XLA Ops:
  7.2 26.2 %copy-start = (bf16[4,192,2048]{2,1,0:T(8,128)(2,1)S(1)}, bf16[4,192,2048]{2,1,0:T(8,128)(2,1)}, u32[]{:S(2)}) copy-start(bf16[4,192,2048]{2,1,0:T(8,128)(2,1)} %param.5) | copy-start | bytes 9437188
  7.2 31.3 %all-gather.2.cloned.1.call-start = ((), (), s32[]{:S(2)}) async-start(), calls=%async_computation.3 | async-start | bytes 1572864 | tf_op jit(solution)/shard_map/all_gather | solution.py:28
  46.9 24.1 %copy-start.3 = (f32[32]{0:T(128)S(1)}, f32[32]{0:T(128)}, u32[]{:S(2)}) copy-start(f32[32]{0:T(128)} %param.9) | copy-start | bytes 388
  49.2 42.6 %copy-start.2 = (bf16[1,16,64]{2,1,0:T(8,128)(2,1)S(1)}, bf16[1,16,64]{2,1,0:T(8,128)(2,1)}, u32[]{:S(2)}) copy-start(bf16[1,16,64]{2,1,0:T(8,128)(2,1)} %param.8) | copy-start | bytes 6148
  65.0 25.6 %all-to-all-start.2 = ((bf16[8,2,192,128]{3,2,1,0:T(8,128)(2,1)}), bf16[8,2,192,128]{3,2,1,0:T(8,128)(2,1)}, u32[]{:S(2)}, u32[]{:S(2)}) async-start(bf16[8,2,192,128]{3,2,1,0:T(8,128)(2,1)} %bitcast.52), calls=%async_computation.2 | async-start | bytes 1572864 | tf_op jit(solution)/shard_map/all_to_all | solution.py:39
  91.8 0.9 copy-start.1
Sparse Core Ops, SparseCore 0:
  9.5 28.9 all-gather.1
